TPU v7x, 32 devices: a whole 2x2x4 slice. The times are simulated.
32 devices in a mesh: sp: 4 (over z), fs: 4 (over y, x), tp: 2 (over core).
Axes of the slice: x: 2, y: 2, z: 4, core: 2. Of those that a mesh axis runs over, the one named last changes fastest.
Arguments:
- tokens: bfloat16 [8192, 2048], P(('fs', 'sp')), parts along dimension 0, may hold values from -6 to 6
- norm_gain: float32 [2048], replicated, may hold values from 0.1 to 1.9
- state_gate: bfloat16 [2048, 1024], P('sp', 'tp'), may hold values from -0.125 to 0.125
- state_value: bfloat16 [2048, 1024], P('sp', 'tp'), may hold values from -0.125 to 0.125
- state_keys: bfloat16 [2048, 1024], P('sp', 'tp'), may hold values from -0.125 to 0.125
- state_query: bfloat16 [2048, 1024], P('sp', 'tp'), may hold values from -0.125 to 0.125
- state_step: bfloat16 [2048, 16], replicated, may hold values from -0.125 to 0.125
- state_rate: float32 [16], P('tp'), may hold values from 0 to 1, as said below
- state_jumps: float32 [8192, 16], P(('fs', 'sp'), 'tp'), parts along dimension 0, may hold values from -3 to 0
- state_gain: float32 [1024], P('tp'), may hold values from 0.1 to 1.9
- filter_value: bfloat16 [5, 1024], P(None, 'tp'), may hold values from -2.5 to 2.5
- filter_keys: bfloat16 [5, 1024], P(None, 'tp'), may hold values from -2.5 to 2.5
- filter_query: bfloat16 [5, 1024], P(None, 'tp'), may hold values from -2.5 to 2.5
- window_query: bfloat16 [2048, 2048], P('sp', 'tp'), may hold values from -64 to 64
- window_keys: bfloat16 [2048, 1024], P('sp', 'tp'), may hold values from -1 to 1
- window_values: bfloat16 [2048, 1024], P('sp', 'tp'), may hold values from -0.125 to 0.125
- window_sink: float32 [16], P('tp'), may hold values from 2.5 to 5.5
- state_output: bfloat16 [1024, 2048], P('tp', 'sp'), may hold values from -0.1875 to 0.1875
- window_output: bfloat16 [2048, 2048], P('tp', 'sp'), may hold values from -2 to 2
Outputs:
- mixed: bfloat16 [8192, 2048], P(('fs', 'sp', 'tp')), parts along dimension 0
There are 4 independent parts, one for each index of `fs`. A program takes and returns all parts, laid end to end along the dimension named above; an argument that names none is the same for every part. Nothing has to cross between parts.
Inputs may be any that keep to these rules, and one draw needn't show every extreme that they name: `state_rate`: a positive rate for each head.
All inputs are finite; a program needn't handle non-finite values.
Results may differ from a plain program's by a relative error of at most 0.015.
The roundings to bfloat16 on the way count: a program that leaves them out, or rounds other values in their place, can miss the bound.
Values may be sent and summed in bfloat16 or wider, within the bound.
A program may use at most 64 MiB of HBM per device.

v0:
```python
import jax
import jax.numpy as jnp
from jax import lax
from jax.sharding import PartitionSpec as P

STATE_SIZE = 128
HEAD_DIM = 128
WINDOW = 128
BLOCK = 128
GRID_WIDTH = 64


def extended(cells, sides, width):
    for axis, dim in sides:
        count = lax.axis_size(axis)
        ends = count - 1
        head = lax.slice_in_dim(cells, 0, width, axis=dim)
        tail = lax.slice_in_dim(cells, cells.shape[dim] - width, cells.shape[dim], axis=dim)
        cells = jnp.concatenate(
            [
                lax.ppermute(tail, axis, [(i, (i + 1) % count) for i in range(ends)]),
                cells,
                lax.ppermute(head, axis, [((i + 1) % count, i) for i in range(ends)]),
            ],
            axis=dim,
        )
    return cells


def rotate_grid(vectors, positions, grid_width):
    head_dim = vectors.shape[-1]
    quarter = head_dim // 4
    half_dim = head_dim // 2
    inverse = 10000.0 ** (-jnp.arange(quarter, dtype=jnp.float32) / quarter)
    grid_row = (positions // grid_width).astype(jnp.float32)
    grid_col = (positions % grid_width).astype(jnp.float32)
    angle_row = grid_row[:, None] * inverse[None, :]
    angle_col = grid_col[:, None] * inverse[None, :]
    angles = jnp.concatenate([angle_row, angle_row, angle_col, angle_col], axis=-1)[:, None, :]
    first_half = vectors[..., :half_dim]
    second = vectors[..., half_dim:]
    turned = jnp.concatenate(
        [
            -first_half[..., quarter:],
            first_half[..., :quarter],
            -second[..., quarter:],
            second[..., :quarter],
        ],
        axis=-1,
    )
    return (
        vectors.astype(jnp.float32) * jnp.cos(angles) + turned.astype(jnp.float32) * jnp.sin(angles)
    ).astype(jnp.bfloat16)


def window_attend(query_rows, keys_pad, values_pad, sink_logits, key_start, total_len, window):
    row_count, query_heads, head_dim = query_rows.shape
    kv_heads = keys_pad.shape[1]
    group_size = query_heads // kv_heads
    block_count = row_count // window
    query_blocks = query_rows.reshape(block_count, window, kv_heads, group_size, head_dim)
    key_split = keys_pad.reshape(block_count + 2, window, kv_heads, head_dim)
    value_split = values_pad.reshape(block_count + 2, window, kv_heads, head_dim)
    key_band = jnp.concatenate([key_split[:-2], key_split[1:-1], key_split[2:]], axis=1)
    value_band = jnp.concatenate([value_split[:-2], value_split[1:-1], value_split[2:]], axis=1)
    scores = jnp.einsum(
        "kihgd,kjhd->khgij", query_blocks, key_band, preferred_element_type=jnp.float32
    ) * head_dim ** (-0.5)
    query_pos = jnp.arange(window)[:, None]
    band_pos = jnp.arange(3 * window)[None, :]
    within = jnp.abs(band_pos - window - query_pos) <= window
    key_pos = (
        key_start + jnp.arange(block_count)[:, None] * window + jnp.arange(3 * window)[None, :]
    )
    inside = (key_pos >= 0) & (key_pos < total_len)
    valid_pair = (within[None] & inside[:, None, :])[:, None, None]
    sink_logit = sink_logits.reshape(kv_heads, group_size)[None, :, :, None, None]
    masked = jnp.where(valid_pair, scores, -1e30)
    ceiling = jnp.maximum(jnp.max(masked, axis=-1, keepdims=True), sink_logit)
    weights = jnp.where(valid_pair, jnp.exp(masked - ceiling), 0.0)
    denominator = jnp.exp(sink_logit - ceiling) + jnp.sum(weights, axis=-1, keepdims=True)
    weights_bf = (weights / denominator).astype(jnp.bfloat16)
    mixed_rows = jnp.einsum(
        "khgij,kjhd->kihgd", weights_bf, value_band, preferred_element_type=jnp.float32
    )
    return mixed_rows.reshape(row_count, query_heads * head_dim).astype(jnp.bfloat16)


def block_terms(query_rows, key_rows, value_rows, log_rows, block_len):
    row_count, group_count, state_size = query_rows.shape
    head_ratio, head_dim = (value_rows.shape[2], value_rows.shape[3])
    block_count = row_count // block_len
    query_blocks = query_rows.reshape(block_count, block_len, group_count, state_size)
    key_blocks = key_rows.reshape(block_count, block_len, group_count, state_size)
    value_blocks = value_rows.reshape(block_count, block_len, group_count, head_ratio, head_dim)
    decay_cum = jnp.cumsum(
        log_rows.reshape(block_count, block_len, group_count, head_ratio), axis=1
    )
    decay_total = decay_cum[:, -1]
    gram_block = jnp.einsum(
        "kign,kjgn->kgij", query_blocks, key_blocks, preferred_element_type=jnp.float32
    )
    cum_heads = jnp.moveaxis(decay_cum, 1, 3)
    distance = jnp.abs(cum_heads[..., :, None] - cum_heads[..., None, :])
    pair_weight = (gram_block[:, :, None] * jnp.exp(-distance)).astype(jnp.bfloat16)
    near_terms = jnp.einsum(
        "kgrij,kjgrp->kigrp", pair_weight, value_blocks, preferred_element_type=jnp.float32
    )
    keys_after = (
        key_blocks[:, :, :, None, :] * jnp.exp(decay_total[:, None] - decay_cum)[..., None]
    ).astype(jnp.bfloat16)
    keys_before = (key_blocks[:, :, :, None, :] * jnp.exp(decay_cum)[..., None]).astype(
        jnp.bfloat16
    )
    state_after = jnp.einsum(
        "kjgrn,kjgrp->kgrnp", keys_after, value_blocks, preferred_element_type=jnp.float32
    )
    state_before = jnp.einsum(
        "kjgrn,kjgrp->kgrnp", keys_before, value_blocks, preferred_element_type=jnp.float32
    )
    before = jnp.cumsum(decay_total, axis=0) - decay_total
    overall = jnp.sum(decay_total, axis=0)
    after_sum = overall[None] - before - decay_total
    block_order = jnp.arange(block_count)
    earlier_mask = (block_order[None, :] < block_order[:, None])[:, :, None, None]
    later_mask = (block_order[None, :] > block_order[:, None])[:, :, None, None]
    gap_fwd = before[:, None] - before[None, :] - decay_total[None, :]
    gap_bwd = before[None, :] - before[:, None] - decay_total[:, None]
    weight_fwd = jnp.where(earlier_mask, jnp.exp(jnp.minimum(gap_fwd, 0.0)), 0.0)
    weight_bwd = jnp.where(later_mask, jnp.exp(jnp.minimum(gap_bwd, 0.0)), 0.0)
    carried_fwd = jnp.einsum(
        "abgr,bgrnp->agrnp", weight_fwd, state_after, precision=lax.Precision.HIGHEST
    )
    carried_bwd = jnp.einsum(
        "abgr,bgrnp->agrnp", weight_bwd, state_before, precision=lax.Precision.HIGHEST
    )
    summary_fwd = jnp.einsum(
        "agr,agrnp->grnp", jnp.exp(after_sum), state_after, precision=lax.Precision.HIGHEST
    )
    summary_bwd = jnp.einsum(
        "agr,agrnp->grnp", jnp.exp(before), state_before, precision=lax.Precision.HIGHEST
    )
    pieces = (
        near_terms,
        carried_fwd,
        carried_bwd,
        decay_cum,
        decay_total,
        before,
        after_sum,
        query_blocks,
    )
    return (pieces, (summary_fwd, summary_bwd, overall))


def finish_terms(pieces, incoming_fwd, incoming_bwd):
    (
        near_terms,
        carried_fwd,
        carried_bwd,
        decay_cum,
        decay_total,
        before,
        after_sum,
        query_blocks,
    ) = pieces
    total_fwd = carried_fwd + jnp.exp(before)[..., None, None] * incoming_fwd[None]
    total_bwd = carried_bwd + jnp.exp(after_sum)[..., None, None] * incoming_bwd[None]
    query_wide = query_blocks.astype(jnp.float32)
    read_fwd = jnp.einsum(
        "kign,kgrnp->kigrp", query_wide, total_fwd, precision=lax.Precision.HIGHEST
    )
    read_bwd = jnp.einsum(
        "kign,kgrnp->kigrp", query_wide, total_bwd, precision=lax.Precision.HIGHEST
    )
    combined = (
        near_terms
        + jnp.exp(decay_cum)[..., None] * read_fwd
        + jnp.exp(decay_total[:, None] - decay_cum)[..., None] * read_bwd
    )
    block_count, block_len, group_count, head_ratio, head_dim = combined.shape
    return combined.reshape(block_count * block_len, group_count, head_ratio, head_dim)


def combine_all(gathered_states, own_index):
    after_all, before_all, logs_all = gathered_states
    device_count = logs_all.shape[0]
    cum_incl = jnp.cumsum(logs_all, axis=0)
    cum_excl = cum_incl - logs_all
    device_order = jnp.arange(device_count)
    picker = (device_order == own_index).astype(jnp.float32)[:, None, None]
    own_incl = jnp.sum(picker * cum_incl, axis=0)
    own_excl = jnp.sum(picker * cum_excl, axis=0)
    lower_mask = (device_order < own_index)[:, None, None]
    higher_mask = (device_order > own_index)[:, None, None]
    weight_fwd = jnp.where(lower_mask, jnp.exp(jnp.minimum(own_excl[None] - cum_incl, 0.0)), 0.0)
    weight_bwd = jnp.where(higher_mask, jnp.exp(jnp.minimum(cum_excl - own_incl[None], 0.0)), 0.0)
    incoming_fwd = jnp.einsum(
        "dgr,dgrnp->grnp", weight_fwd, after_all, precision=lax.Precision.HIGHEST
    )
    incoming_bwd = jnp.einsum(
        "dgr,dgrnp->grnp", weight_bwd, before_all, precision=lax.Precision.HIGHEST
    )
    return (incoming_fwd, incoming_bwd)


def shards(
    tokens,
    norm_gain,
    state_gate,
    state_value,
    state_keys,
    state_query,
    state_step,
    state_rate,
    state_jumps,
    state_gain,
    filter_value,
    filter_keys,
    filter_query,
    window_query,
    window_keys,
    window_values,
    window_sink,
    state_output,
    window_output,
):
    row_count = tokens.shape[0]
    rows_wide = tokens.astype(jnp.float32)
    normed = (
        rows_wide
        * lax.rsqrt(jnp.mean(rows_wide * rows_wide, axis=-1, keepdims=True) + 1e-06)
        * norm_gain
    ).astype(jnp.bfloat16)
    gathered = (
        lax.all_gather(state_gate, "sp", axis=0, tiled=True),
        lax.all_gather(state_value, "sp", axis=0, tiled=True),
        lax.all_gather(state_keys, "sp", axis=0, tiled=True),
        lax.all_gather(state_query, "sp", axis=0, tiled=True),
        lax.all_gather(window_query, "sp", axis=0, tiled=True),
        lax.all_gather(window_keys, "sp", axis=0, tiled=True),
        lax.all_gather(window_values, "sp", axis=0, tiled=True),
        lax.all_gather(state_output, "sp", axis=1, tiled=True),
        lax.all_gather(window_output, "sp", axis=1, tiled=True),
    )
    projected = [
        jnp.dot(normed, matrix, preferred_element_type=jnp.float32) for matrix in gathered[:7]
    ]
    out_state = gathered[7]
    out_window = gathered[8]
    gate_rows, value_pre, keys_pre, query_pre, query_raw, keys_raw, values_rows = [
        result.astype(jnp.bfloat16) for result in projected
    ]
    head_local = state_rate.shape[0]
    group_local = keys_pre.shape[1] // STATE_SIZE
    head_dim = value_pre.shape[1] // head_local
    head_ratio = head_local // group_local
    step_cols = lax.dynamic_slice_in_dim(
        state_step, lax.axis_index("tp") * head_local, head_local, 1
    )
    step_rows = jax.nn.softplus(jnp.dot(normed, step_cols, preferred_element_type=jnp.float32))
    log_decay = -state_rate[None, :] * step_rows + state_jumps
    half_width = filter_value.shape[0] // 2
    stacked = jnp.concatenate([value_pre, keys_pre, query_pre], axis=-1)
    padded = extended(stacked, (("sp", 0),), half_width)
    filters = jnp.concatenate([filter_value, filter_keys, filter_query], axis=-1).astype(
        jnp.float32
    )
    filtered = jnp.zeros(stacked.shape, jnp.float32)
    for offset in range(filters.shape[0]):
        filtered = (
            filtered + padded[offset : offset + row_count].astype(jnp.float32) * filters[offset]
        )
    value_cols = value_pre.shape[1]
    key_cols = keys_pre.shape[1]
    inner_rows = (
        jax.nn.silu(filtered[:, :value_cols]).reshape(row_count, head_local, head_dim)
        * step_rows[..., None]
    )
    scan_values = inner_rows.astype(jnp.bfloat16).reshape(
        row_count, group_local, head_ratio, head_dim
    )
    scan_keys = (
        filtered[:, value_cols : value_cols + key_cols]
        .astype(jnp.bfloat16)
        .reshape(row_count, group_local, STATE_SIZE)
    )
    scan_query = (
        filtered[:, value_cols + key_cols :]
        .astype(jnp.bfloat16)
        .reshape(row_count, group_local, STATE_SIZE)
    )
    pieces, summaries = block_terms(
        scan_query,
        scan_keys,
        scan_values,
        log_decay.reshape(row_count, group_local, head_ratio),
        BLOCK,
    )
    summary_fwd, summary_bwd, overall = summaries
    gathered_states = (
        lax.all_gather(summary_fwd[None].astype(jnp.bfloat16), "sp", axis=0, tiled=True).astype(
            jnp.float32
        ),
        lax.all_gather(summary_bwd[None].astype(jnp.bfloat16), "sp", axis=0, tiled=True).astype(
            jnp.float32
        ),
        lax.all_gather(overall[None].astype(jnp.bfloat16), "sp", axis=0, tiled=True).astype(
            jnp.float32
        ),
    )
    incoming_fwd, incoming_bwd = combine_all(gathered_states, lax.axis_index("sp"))
    scan_out = finish_terms(pieces, incoming_fwd, incoming_bwd).reshape(
        row_count, head_local * head_dim
    )
    gated_rows = scan_out * jax.nn.silu(gate_rows.astype(jnp.float32))
    per_head = gated_rows.reshape(row_count, head_local, head_dim)
    state_mix = (
        (
            per_head
            * lax.rsqrt(jnp.mean(per_head * per_head, axis=-1, keepdims=True) + 1e-06)
            * state_gain.reshape(head_local, head_dim)
        )
        .astype(jnp.bfloat16)
        .reshape(row_count, head_local * head_dim)
    )
    query_heads = window_sink.shape[0]
    kv_heads = keys_raw.shape[1] // HEAD_DIM
    kv_width = kv_heads * HEAD_DIM
    positions = lax.axis_index("sp") * row_count + jnp.arange(row_count, dtype=jnp.int32)
    query_rot = rotate_grid(
        query_raw.reshape(row_count, query_heads, HEAD_DIM), positions, GRID_WIDTH
    )
    keys_rot = rotate_grid(keys_raw.reshape(row_count, kv_heads, HEAD_DIM), positions, GRID_WIDTH)
    pair_rows = jnp.concatenate([keys_rot.reshape(row_count, kv_width), values_rows], axis=-1)
    padded_pair = extended(pair_rows, (("sp", 0),), WINDOW)
    keys_pad = padded_pair[:, :kv_width].reshape(-1, kv_heads, HEAD_DIM)
    values_pad = padded_pair[:, kv_width:].reshape(-1, kv_heads, HEAD_DIM)
    window_mix = window_attend(
        query_rot,
        keys_pad,
        values_pad,
        window_sink,
        lax.axis_index("sp") * row_count - WINDOW,
        lax.axis_size("sp") * row_count,
        WINDOW,
    )
    return lax.psum_scatter(
        (
            jnp.dot(state_mix, out_state, preferred_element_type=jnp.float32)
            + jnp.dot(window_mix, out_window, preferred_element_type=jnp.float32)
        ).astype(jnp.bfloat16),
        "tp",
        scatter_dimension=0,
        tiled=True,
    )


def solution(mesh):
    placed = (
        P(("fs", "sp"), None),
        P(),
        P("sp", "tp"),
        P("sp", "tp"),
        P("sp", "tp"),
        P("sp", "tp"),
        P(),
        P("tp"),
        P(("fs", "sp"), "tp"),
        P("tp"),
        P(None, "tp"),
        P(None, "tp"),
        P(None, "tp"),
        P("sp", "tp"),
        P("sp", "tp"),
        P("sp", "tp"),
        P("tp"),
        P("tp", "sp"),
        P("tp", "sp"),
    )
    return jax.shard_map(
        shards, mesh=mesh, in_specs=placed, out_specs=P(("fs", "sp", "tp"), None), check_vma=False
    )
```

profile of v0, /device:TPU:0, one launch (start us, length us, event | category | flops | bytes accessed | tf_op | source)
XLA Modules:
  0.0 539.9 jit_solution(15252986102147311242)
XLA Ops:
  20.1 13.3 %all-gather.3 = bf16[4,4,2]{1,2,0:T(2,128)(2,1)S(1)} all-gather(bf16[1,4,2]{1,2,0:T(2,128)(2,1)S(1)} %convert_bitcast_fusion), channel_id=2, replica_groups=mesh['sp'=4,'fs'=4,'tp'=2] {'sp'}, dimensions={0}, use_global_device_ids=true | all-gather | bytes 80 | tf_op jit(solution)/shard_map/all_gather | solution.py:308
  40.1 17.2 %all-gather.24.cloned.1.call-done = bf16[2048,512]{1,0:T(8,128)(2,1)} async-done(((bf16[512,512]{1,0:T(8,128)(2,1)}), bf16[2048,512]{1,0:T(8,128)(2,1)}) %all-gather.24.cloned.1.call-update) | async-done | bytes 2097168 | tf_op jit(solution)/shard_map/all_gather | solution.py:241
  60.4 43.0 %all-gather.18.cloned.1.call-done = bf16[2048,512]{1,0:T(8,128)(2,1)} async-done(((bf16[512,512]{1,0:T(8,128)(2,1)}), bf16[2048,512]{1,0:T(8,128)(2,1)}) %all-gather.18.cloned.1.call-update) | async-done | bytes 2097168 | tf_op jit(solution)/shard_map/all_gather | solution.py:239
  103.4 3.6 convolution_convert_fusion.4
  107.0 42.5 %all-gather.16.cloned.1.call-done = bf16[2048,512]{1,0:T(8,128)(2,1)} async-done(((bf16[512,512]{1,0:T(8,128)(2,1)}), bf16[2048,512]{1,0:T(8,128)(2,1)}) %all-gather.16.cloned.1.call-update) | async-done | bytes 2097168 | tf_op jit(solution)/shard_map/all_gather | solution.py:238
  149.5 3.6 convolution_convert_fusion.5
  153.1 42.3 %all-gather.14.cloned.1.call-done = bf16[2048,512]{1,0:T(8,128)(2,1)} async-done(((bf16[512,512]{1,0:T(8,128)(2,1)}), bf16[2048,512]{1,0:T(8,128)(2,1)}) %all-gather.14.cloned.1.call-update) | async-done | bytes 2097168 | tf_op jit(solution)/shard_map/all_gather | solution.py:237
  195.4 3.6 convolution_convert_fusion.6
  205.2 44.7 %all-gather.26.cloned.1.call-done = bf16[2048,512]{1,0:T(8,128)(2,1)} async-done(((bf16[512,512]{1,0:T(8,128)(2,1)}), bf16[2048,512]{1,0:T(8,128)(2,1)}) %all-gather.26.cloned.1.call-update) | async-done | bytes 2097168 | tf_op jit(solution)/shard_map/all_gather | solution.py:242
  249.9 3.6 convolution_convert_fusion.1
  261.8 5.9 %maximum_maximum_fusion = (bf16[514,1536]{0,1:T(8,128)(2,1)S(1)}, bf16[514,1536]{0,1:T(8,128)(2,1)S(1)}) fusion(bf16[512,512]{0,1:T(8,128)(2,1)S(1)} %convolution_convert_fusion.4, bf16[512,512]{0,1:T(8,128)(2,1)S(1)} %convolution_convert_fusion.5, bf16[512,512]{0,1:T(8,128)(2,1)S(1)} %convolution_convert_fusion.6, bf16[2,1536]{0,1:T(8,128)(2,1)} %collective-permute-done, ...), kind=kLoop, calls=%fused_computation.19 | loop fusion | flops 12632064 | bytes 4743168 | tf_op jit(solution)/shard_map/concatenate | solution.py:19
  267.7 5.8 %fusion.122 = (bf16[512,1536]{0,1:T(8,128)(2,1)}, f32[512,1536]{0,1:T(8,128)S(1)}) fusion(f32[1536]{0:T(1024)S(1)} %get-tuple-element.9, bf16[514,1536]{0,1:T(8,128)(2,1)S(1)} %get-tuple-element.19, f32[1536]{0:T(1024)S(1)} %get-tuple-element.6, f32[1536]{0:T(1024)S(1)} %get-tuple-element.7, bf16[512,512]{0,1:T(8,128)(2,1)S(1)} %convolution_convert_fusion.4, ...), kind=kLoop, calls=%fused_computation.221 | loop fusion | flops 15728640 | bytes 12613632 | tf_op jit(solution)/shard_map/convert.2
  284.0 23.4 %all-gather.1 = bf16[16,2,128,64]{2,3,1,0:T(8,128)(2,1)S(1)} all-gather(bf16[4,2,128,64]{2,3,1,0:T(8,128)(2,1)S(1)} %get-tuple-element.59), channel_id=3, replica_groups=mesh['sp'=4,'fs'=4,'tp'=2] {'sp'}, dimensions={0}, use_global_device_ids=true | all-gather | bytes 655360 | tf_op jit(solution)/shard_map/all_gather | solution.py:302
  308.5 16.1 %all-gather.2 = bf16[16,2,128,64]{2,3,1,0:T(8,128)(2,1)S(1)} all-gather(bf16[4,2,128,64]{2,3,1,0:T(8,128)(2,1)S(1)} %get-tuple-element.62), channel_id=4, replica_groups=mesh['sp'=4,'fs'=4,'tp'=2] {'sp'}, dimensions={0}, use_global_device_ids=true | all-gather | bytes 655360 | tf_op jit(solution)/shard_map/all_gather | solution.py:305
  334.8 3.9 bitcast_reduce_fusion
  346.6 45.2 %all-gather.28.cloned.1.call-done = bf16[2048,1024]{1,0:T(8,128)(2,1)} async-done(((bf16[512,1024]{1,0:T(8,128)(2,1)}), bf16[2048,1024]{1,0:T(8,128)(2,1)}) %all-gather.28.cloned.1.call-update) | async-done | bytes 4194320 | tf_op jit(solution)/shard_map/all_gather | solution.py:240
  391.8 5.4 %convolution_convert_fusion = bf16[512,1024]{1,0:T(8,128)(2,1)S(1)} fusion(bf16[2048,1024]{1,0:T(8,128)(2,1)} %all-gather.28.cloned.1.call-done, bf16[512,2048]{1,0:T(8,128)(2,1)} %param.19, f32[2048]{0:T(1024)S(1)} %copy-done.23, f32[512]{0:T(512)S(1)} %copy-done.17), kind=kOutput, calls=%fused_computation.34 | convolution fusion | flops 2152202240 | bytes 7350272 | tf_op jit(solution)/shard_map/dot_general | solution.py:247
  397.2 3.1 reshape.412
  408.4 5.3 fusion
  419.9 52.7 %all-gather.30.cloned.1.call-done = bf16[1024,2048]{1,0:T(8,128)(2,1)} async-done(((bf16[1024,512]{1,0:T(8,128)(2,1)}), bf16[1024,2048]{1,0:T(8,128)(2,1)}) %all-gather.30.cloned.1.call-update) | async-done | bytes 4194320 | tf_op jit(solution)/shard_map/all_gather | solution.py:244
  472.6 6.5 %fusion.128 = f32[512,2048]{1,0:T(8,128)} fusion(bf16[512,1024]{1,0:T(8,128)(2,1)S(1)} %convert_element_type.224, bf16[1024,2048]{1,0:T(8,128)(2,1)} %all-gather.30.cloned.1.call-done), kind=kOutput, calls=%fused_computation.227 | convolution fusion | flops 2147483648 | bytes 9437184 | tf_op jit(solution)/shard_map/dot_general | solution.py:351
  479.2 39.2 %all-gather.22.cloned.1.call-done = bf16[512,2048]{1,0:T(8,128)(2,1)} async-done(((bf16[512,512]{1,0:T(8,128)(2,1)}), bf16[512,2048]{1,0:T(8,128)(2,1)}) %all-gather.22.cloned.1.call-update) | async-done | bytes 2097168 | tf_op jit(solution)/shard_map/all_gather | solution.py:243
  518.4 5.5 %add_convert_fusion = bf16[512,2048]{1,0:T(8,128)(2,1)} fusion(f32[512,2048]{1,0:T(8,128)} %fusion.128, bf16[512,512]{0,1:T(8,128)(2,1)S(1)} %fusion.41, bf16[512,2048]{1,0:T(8,128)(2,1)} %all-gather.22.cloned.1.call-done), kind=kOutput, calls=%fused_computation.10 | convolution fusion | flops 1075838976 | bytes 8912896 | tf_op jit(solution)/shard_map/dot_general | solution.py:350
  523.9 8.7 %reduce-scatter.2.cloned.1.call-done = bf16[256,2048]{1,0:T(8,128)(2,1)} async-done(((bf16[512,2048]{1,0:T(8,128)(2,1)}), bf16[256,2048]{1,0:T(8,128)(2,1)}) %reduce-scatter.2.cloned.1.call-update) | async-done | bytes 1048592 | tf_op jit(solution)/shard_map/reduce_scatter | solution.py:348
  (184 shorter events, 81.0 us)
Async XLA Ops:
  6.5 6.9 %copy-start = (bf16[2048,16]{0,1:T(8,128)(2,1)S(1)}, bf16[2048,16]{0,1:T(8,128)(2,1)}, u32[]{:S(2)}) copy-start(bf16[2048,16]{0,1:T(8,128)(2,1)} %param.25) | copy-start | bytes 196612
  6.5 50.8 %all-gather.24.cloned.1.call-start = ((), (), s32[]{:S(2)}) async-start(), calls=%async_computation.6 | async-start | bytes 2621440 | tf_op jit(solution)/shard_map/all_gather | solution.py:241
  7.3 96.2 %all-gather.18.cloned.1.call-start = ((), (), s32[]{:S(2)}) async-start(), calls=%async_computation.3 | async-start | bytes 2621440 | tf_op jit(solution)/shard_map/all_gather | solution.py:239
  8.0 141.5 %all-gather.16.cloned.1.call-start = ((), (), s32[]{:S(2)}) async-start(), calls=%async_computation.2 | async-start | bytes 2621440 | tf_op jit(solution)/shard_map/all_gather | solution.py:238
  8.8 186.6 %all-gather.14.cloned.1.call-start = ((), (), s32[]{:S(2)}) async-start(), calls=%async_computation.1 | async-start | bytes 2621440 | tf_op jit(solution)/shard_map/all_gather | solution.py:237
  9.4 240.6 %all-gather.26.cloned.1.call-start = ((), (), s32[]{:S(2)}) async-start(), calls=%async_computation.7 | async-start | bytes 2621440 | tf_op jit(solution)/shard_map/all_gather | solution.py:242
  9.9 324.9 %all-gather.20.cloned.1.call-start = ((), (), s32[]{:S(2)}) async-start(), calls=%async_computation.4 | async-start | bytes 2621440 | tf_op jit(solution)/shard_map/all_gather | solution.py:236
  10.5 381.2 %all-gather.28.cloned.1.call-start = ((), (), s32[]{:S(2)}) async-start(), calls=%async_computation.8 | async-start | bytes 5242880 | tf_op jit(solution)/shard_map/all_gather | solution.py:240
  11.3 461.3 %all-gather.30.cloned.1.call-start = ((), (), s32[]{:S(2)}) async-start(), calls=%async_computation.9 | async-start | bytes 5242880 | tf_op jit(solution)/shard_map/all_gather | solution.py:244
  12.0 506.4 %all-gather.22.cloned.1.call-start = ((), (), s32[]{:S(2)}) async-start(), calls=%async_computation.5 | async-start | bytes 2621440 | tf_op jit(solution)/shard_map/all_gather | solution.py:243
  12.8 519.8 %reduce-scatter.2.cloned.1.call-start = ((), (), s32[]{:S(2)}) async-start(), calls=%async_computation.10 | async-start | bytes 3145728 | tf_op jit(solution)/shard_map/reduce_scatter | solution.py:348
  20.1 37.3 %copy-start.4 = (bf16[512,2048]{1,0:T(8,128)(2,1)S(1)}, bf16[512,2048]{1,0:T(8,128)(2,1)}, u32[]{:S(2)}) copy-start(bf16[512,2048]{1,0:T(8,128)(2,1)} %param.19) | copy-start | bytes 6291460
  40.1 63.3 %copy-start.17 = (f32[512]{0:T(512)S(1)}, f32[512]{0:T(512)}, u32[]{:S(2)}) copy-start(f32[512]{0:T(512)} %copy-done.16) | copy-start | bytes 6148
  40.1 63.3 %copy-start.23 = (f32[2048]{0:T(1024)S(1)}, f32[2048]{0:T(1024)}, u32[]{:S(2)}) copy-start(f32[2048]{0:T(1024)} %param.20) | copy-start | bytes 24580
  200.2 61.6 %collective-permute-start = (bf16[2,1536]{0,1:T(8,128)(2,1)}, bf16[2,1536]{0,1:T(8,128)(2,1)}, u32[]{:S(2)}, u32[]{:S(2)}) collective-permute-start(bf16[2,1536]{0,1:T(8,128)(2,1)} %get-tuple-element.20), channel_id=1, source_target_pairs={{0,8},{8,16},{16,24},{1,9},{9,17},{17,25},{2,10},{10,18},{18,26},{... | collective-permute-start | bytes 18440 | tf_op jit(solution)/shard_map/ppermute | solution.py:21
  203.0 58.8 %collective-permute-start.1 = (bf16[2,1536]{0,1:T(8,128)(2,1)}, bf16[2,1536]{0,1:T(8,128)(2,1)}, u32[]{:S(2)}, u32[]{:S(2)}) collective-permute-start(bf16[2,1536]{0,1:T(8,128)(2,1)} %get-tuple-element.21), channel_id=1, source_target_pairs={{8,0},{16,8},{24,16},{9,1},{17,9},{25,17},{10,2},{18,10},{26,18},{... | collective-permute-start | bytes 18440 | tf_op jit(solution)/shard_map/ppermute | solution.py:23
  255.4 83.5 %collective-permute-start.2 = (bf16[128,1024]{0,1:T(8,128)(2,1)}, bf16[128,1024]{0,1:T(8,128)(2,1)S(1)}, u32[]{:S(2)}, u32[]{:S(2)}) collective-permute-start(bf16[128,1024]{0,1:T(8,128)(2,1)} %get-tuple-element.37), channel_id=1, source_target_pairs={{0,8},{8,16},{16,24},{1,9},{9,17},{17,25},{2,10},{10,18},{18,26},{... | collective-permute-start | bytes 786440 | tf_op jit(solution)/shard_map/ppermute | solution.py:21
  257.4 81.5 %collective-permute-start.3 = (bf16[128,1024]{0,1:T(8,128)(2,1)}, bf16[128,1024]{0,1:T(8,128)(2,1)}, u32[]{:S(2)}, u32[]{:S(2)}) collective-permute-start(bf16[128,1024]{0,1:T(8,128)(2,1)} %get-tuple-element.38), channel_id=1, source_target_pairs={{8,0},{16,8},{24,16},{9,1},{17,9},{25,17},{10,2},{18,10},{26,18},{... | collective-permute-start | bytes 786440 | tf_op jit(solution)/shard_map/ppermute | solution.py:23
  282.8 41.7 %copy-start.6 = (f32[4,4,128,128]{3,2,1,0:T(8,128)S(1)}, f32[4,4,128,128]{3,2,1,0:T(8,128)}, u32[]{:S(2)}) copy-start(f32[4,4,128,128]{3,2,1,0:T(8,128)} %fusion.56) | copy-start | bytes 3145732
  282.9 41.7 %copy-start.12 = (f32[4,4,2,128]{3,2,1,0:T(2,128)S(1)}, f32[4,4,2,128]{3,2,1,0:T(2,128)}, u32[]{:S(2)}) copy-start(f32[4,4,2,128]{3,2,1,0:T(2,128)} %copy.184) | copy-start | bytes 49156
  308.5 17.8 %copy-start.14 = (f32[4,4,2]{0,2,1:T(2,128)S(1)}, f32[4,4,2]{0,2,1:T(2,128)}, u32[]{:S(2)}) copy-start(f32[4,4,2]{0,2,1:T(2,128)} %copy.195) | copy-start | bytes 388
  308.5 17.8 %copy-start.20 = (pred[4,4]{1,0:T(4,128)(4,1)S(1)}, pred[4,4]{1,0:T(4,128)(4,1)}, u32[]{:S(2)}) copy-start(pred[4,4]{1,0:T(4,128)(4,1)} %iota_compare_fusion.1) | copy-start | bytes 52
  401.7 6.7 %copy-start.5 = (f32[4,128,4,2,128]{4,3,2,1,0:T(2,128)S(1)}, f32[4,128,4,2,128]{4,3,2,1,0:T(2,128)}, u32[]{:S(2)}) copy-start(f32[4,128,4,2,128]{4,3,2,1,0:T(2,128)} %reshape.412) | copy-start | bytes 6291460
  518.4 14.2 %copy-start.1 = (bf16[2048,16]{0,1:T(8,128)(2,1)S(1)}, bf16[2048,16]{0,1:T(8,128)(2,1)}, u32[]{:S(2)}) copy-start(bf16[2048,16]{0,1:T(8,128)(2,1)} %param.25) | copy-start | bytes 196612
  (15 other events, 52.8 us)
Sparse Core Ops, SparseCore 0:
  8.9 48.4 all-gather.23
  58.9 44.4 all-gather.17
  105.0 44.4 all-gather.15
  150.9 44.4 all-gather.13
  196.8 53.0 all-gather.25
  251.3 58.3 all-gather.19
  311.3 80.3 all-gather.27
  393.3 79.2 all-gather.29
  474.2 44.1 all-gather.21
  524.0 8.5 reduce-scatter.1
where the time goes:
time: 549 us; the launch traced here: 540 us
  waiting for transfers between devices  341 us (62%)
  matrix products  60.4 us (11%)
  blocking collectives  52.7 us (10%)
  local copies, waits for them, and re-layouts  33.6 us (6%)
  other arithmetic  28.8 us (5%)
  between operations  14.7 us (3%)
  starting transfers between devices  8.28 us (2%)
    all_gather x1, waiting for transfers between devices, shards(): lax.all_gather(window_output, 'sp', axis=1, tiled=True)  52.7 us
    all_gather x1, waiting for transfers between devices, shards(): lax.all_gather(window_query, 'sp', axis=0, tiled=True)  45.2 us
    all_gather x1, waiting for transfers between devices, shards(): lax.all_gather(window_values, 'sp', axis=0, tiled=True)  44.7 us
    all_gather x1, waiting for transfers between devices, shards(): lax.all_gather(state_query, 'sp', axis=0, tiled=True)  43 us
    all_gather x1, waiting for transfers between devices, shards(): lax.all_gather(state_keys, 'sp', axis=0, tiled=True)  42.5 us
    all_gather x1, waiting for transfers between devices, shards(): lax.all_gather(state_value, 'sp', axis=0, tiled=True)  42.3 us
    all_gather x1, waiting for transfers between devices, shards(): lax.all_gather(state_output, 'sp', axis=1, tiled=True)  39.2 us
    dot_general x7, matrix products, shards(): jnp.dot(normed, matrix, preferred_element_type=jnp.float32)  26.7 us
  transfers between devices with their start and end apart: 14, of which 9 were waited for; matrix products, arithmetic and copies ran while one was open for 22% of the time, Pallas kernels for 0%

commit v1 on v0

--- a/solution.py
+++ b/solution.py
@@ -8,6 +8,33 @@
 WINDOW = 128
 BLOCK = 128
 GRID_WIDTH = 64
+
+
+def ranges_launch(in_array, in_dim):
+    in_array = jnp.moveaxis(in_array, 0, in_dim)
+    inter = in_array.shape
+    return in_array.reshape(
+        *inter[:in_dim], inter[in_dim] * inter[in_dim + 1], *inter[in_dim + 2 :]
+    )
+
+
+def _choose_screen(x_local, peer_axis):
+    wide_n = jax.lax.axis_size(peer_axis)
+    all_rows = x_local[None]
+    for k0 in range(wide_n.bit_length() - 1):
+        passed = 1 << k0
+        items = []
+        for to_i in [*range(wide_n)]:
+            items.append((to_i, to_i ^ passed))
+        now = jax.lax.ppermute(all_rows, peer_axis, items)
+        high = jnp.stack([all_rows, now], axis=0)
+        side_arr = jax.lax.axis_index(peer_axis) >> k0 & 1
+        all_rows = jnp.where(side_arr == 0, high, high[::-1]).reshape(-1, *x_local.shape)
+    return all_rows
+
+
+def record_attach(m, row_data, dim_i):
+    return ranges_launch(_choose_screen(m, row_data), dim_i)
 
 
 def extended(cells, sides, width):
@@ -236,7 +263,7 @@
         lax.all_gather(state_gate, "sp", axis=0, tiled=True),
         lax.all_gather(state_value, "sp", axis=0, tiled=True),
         lax.all_gather(state_keys, "sp", axis=0, tiled=True),
-        lax.all_gather(state_query, "sp", axis=0, tiled=True),
+        record_attach(state_query, "sp", 0),
         lax.all_gather(window_query, "sp", axis=0, tiled=True),
         lax.all_gather(window_keys, "sp", axis=0, tiled=True),
         lax.all_gather(window_values, "sp", axis=0, tiled=True),

time: 549 us -> 530 us (0.965); the launches traced: 540 us -> 527 us
  waiting for transfers between devices: 341 us -> 301 us
  blocking collectives: 52.7 us -> 73.7 us
    ppermute x0 -> x2, waiting for transfers between devices: none -> 73.2 us  [_choose_screen(): now = jax.lax.ppermute(all_rows, peer_axis, items)]
    all_gather x1 -> x0, waiting for transfers between devices: 43 us -> none  [shards(): lax.all_gather(state_query, 'sp', axis=0, tiled=True)]
    all_gather x1, waiting for transfers between devices: 42.5 us -> 0.02 us  [shards(): lax.all_gather(state_keys, 'sp', axis=0, tiled=True)]
    all_gather x1, blocking collectives: 13.3 us -> 34.2 us  [shards(): lax.all_gather(overall[None].astype(jnp.bfloat16), 'sp', axis=0, tiled=True)]
    all_gather x1, waiting for transfers between devices: 17.2 us -> 0.02 us  [shards(): lax.all_gather(window_keys, 'sp', axis=0, tiled=True)]
    all_gather x1, waiting for transfers between devices: 42.3 us -> 32.2 us  [shards(): lax.all_gather(state_value, 'sp', axis=0, tiled=True)]
  transfers between devices with their start and end apart: 14 -> 15, of which waited for: 9 -> 7; matrix products, arithmetic and copies ran while one was open for 22% -> 23% of each run, Pallas kernels for 0% -> 0%
where the time goes in v1:
time: 530 us; the launch traced here: 527 us
  waiting for transfers between devices  301 us (57%)
  blocking collectives  73.7 us (14%)
  matrix products  58.8 us (11%)
  local copies, waits for them, and re-layouts  34.9 us (7%)
  other arithmetic  32.4 us (6%)
  between operations  14.4 us (3%)
  starting transfers between devices  11.4 us (2%)
    ppermute x2, waiting for transfers between devices, _choose_screen(): now = jax.lax.ppermute(all_rows, peer_axis, items)  73.2 us
    all_gather x1, waiting for transfers between devices, shards(): lax.all_gather(window_output, 'sp', axis=1, tiled=True)  54.2 us
    all_gather x1, waiting for transfers between devices, shards(): lax.all_gather(window_values, 'sp', axis=0, tiled=True)  44.6 us
    all_gather x1, waiting for transfers between devices, shards(): lax.all_gather(window_query, 'sp', axis=0, tiled=True)  44.4 us
    all_gather x1, waiting for transfers between devices, shards(): lax.all_gather(state_output, 'sp', axis=1, tiled=True)  39.2 us
    all_gather x1, blocking collectives, shards(): lax.all_gather(overall[None].astype(jnp.bfloat16), 'sp', axis=0, tiled=True)  34.2 us
    all_gather x1, waiting for transfers between devices, shards(): lax.all_gather(state_value, 'sp', axis=0, tiled=True)  32.2 us
    dot_general x7, matrix products, shards(): jnp.dot(normed, matrix, preferred_element_type=jnp.float32)  25.1 us
  transfers between devices with their start and end apart: 15, of which 7 were waited for; matrix products, arithmetic and copies ran while one was open for 23% of the time, Pallas kernels for 0%

profile of v1, /device:TPU:0, one launch (start us, length us, event | category | flops | bytes accessed | tf_op | source)
XLA Modules:
  0.0 526.5 jit_solution(4646906267845557826)
XLA Ops:
  11.3 3.1 collective-permute-start
  18.5 34.2 %all-gather.3 = bf16[4,4,2]{1,2,0:T(2,128)(2,1)S(1)} all-gather(bf16[1,4,2]{1,2,0:T(2,128)(2,1)S(1)} %convert_bitcast_fusion), channel_id=2, replica_groups=mesh['sp'=4,'fs'=4,'tp'=2] {'sp'}, dimensions={0}, use_global_device_ids=true | all-gather | bytes 80 | tf_op jit(solution)/shard_map/all_gather | solution.py:335
  65.2 73.2 %collective-permute-done.1 = bf16[2,512,512]{2,1,0:T(8,128)(2,1)} collective-permute-done((bf16[2,512,512]{2,1,0:T(8,128)(2,1)}, bf16[2,512,512]{2,1,0:T(8,128)(2,1)}, u32[]{:S(2)}, u32[]{:S(2)}) %collective-permute-start.1) | collective-permute-done | bytes 1048608 | tf_op jit(solution)/shard_map/ppermute | solution.py:29
  142.9 3.9 convolution_convert_fusion.2
  146.9 3.6 convolution_convert_fusion.5
  150.5 32.2 %all-gather.13.cloned.1.call-done = bf16[2048,512]{1,0:T(8,128)(2,1)} async-done(((bf16[512,512]{1,0:T(8,128)(2,1)}), bf16[2048,512]{1,0:T(8,128)(2,1)}) %all-gather.13.cloned.1.call-update) | async-done | bytes 2097168 | tf_op jit(solution)/shard_map/all_gather | solution.py:264
  182.7 3.6 convolution_convert_fusion.6
  187.5 2.8 collective-permute-start.2
  192.5 44.6 %all-gather.23.cloned.1.call-done = bf16[2048,512]{1,0:T(8,128)(2,1)} async-done(((bf16[512,512]{1,0:T(8,128)(2,1)}), bf16[2048,512]{1,0:T(8,128)(2,1)}) %all-gather.23.cloned.1.call-update) | async-done | bytes 2097168 | tf_op jit(solution)/shard_map/all_gather | solution.py:269
  237.2 3.6 convolution_convert_fusion.1
  249.1 5.9 %maximum_maximum_fusion = (bf16[514,1536]{0,1:T(8,128)(2,1)S(1)}, bf16[514,1536]{0,1:T(8,128)(2,1)S(1)}) fusion(bf16[512,512]{0,1:T(8,128)(2,1)S(1)} %convolution_convert_fusion.4, bf16[512,512]{0,1:T(8,128)(2,1)S(1)} %convolution_convert_fusion.5, bf16[512,512]{0,1:T(8,128)(2,1)S(1)} %convolution_convert_fusion.6, ...), kind=kLoop, calls=%fused_computation.21 | loop fusion | flops 12632064 | bytes 4743168 | tf_op jit(solution)/shard_map/concatenate | solution.py:46
  255.0 5.8 %fusion.124 = (bf16[512,1536]{0,1:T(8,128)(2,1)}, f32[512,1536]{0,1:T(8,128)S(1)}) fusion(f32[1536]{0:T(1024)S(1)} %copy-done.17, bf16[514,1536]{0,1:T(8,128)(2,1)S(1)} %get-tuple-element.19, f32[1536]{0:T(1024)S(1)} %copy-done.14, f32[1536]{0:T(1024)S(1)} %copy-done.15, bf16[512,512]{0,1:T(8,128)(2,1)S(1)} %convolution_convert_fusion.4, ...), kind=kLoop, calls=%fused_computation.227 | loop fusion | flops 15728640 | bytes 12613632 | tf_op jit(solution)/shard_map/convert.2
  271.4 23.5 %all-gather.1 = bf16[16,2,128,64]{2,3,1,0:T(8,128)(2,1)S(1)} all-gather(bf16[4,2,128,64]{2,3,1,0:T(8,128)(2,1)S(1)} %get-tuple-element.61), channel_id=3, replica_groups=mesh['sp'=4,'fs'=4,'tp'=2] {'sp'}, dimensions={0}, use_global_device_ids=true | all-gather | bytes 655360 | tf_op jit(solution)/shard_map/all_gather | solution.py:329
  296.0 16.0 %all-gather.2 = bf16[16,2,128,64]{2,3,1,0:T(8,128)(2,1)S(1)} all-gather(bf16[4,2,128,64]{2,3,1,0:T(8,128)(2,1)S(1)} %get-tuple-element.64), channel_id=4, replica_groups=mesh['sp'=4,'fs'=4,'tp'=2] {'sp'}, dimensions={0}, use_global_device_ids=true | all-gather | bytes 655360 | tf_op jit(solution)/shard_map/all_gather | solution.py:332
  323.3 3.5 bitcast_reduce_fusion
  334.7 44.4 %all-gather.25.cloned.1.call-done = bf16[2048,1024]{1,0:T(8,128)(2,1)} async-done(((bf16[512,1024]{1,0:T(8,128)(2,1)}), bf16[2048,1024]{1,0:T(8,128)(2,1)}) %all-gather.25.cloned.1.call-update) | async-done | bytes 4194320 | tf_op jit(solution)/shard_map/all_gather | solution.py:267
  379.1 5.4 %convolution_convert_fusion = bf16[512,1024]{1,0:T(8,128)(2,1)S(1)} fusion(bf16[2048,1024]{1,0:T(8,128)(2,1)} %all-gather.25.cloned.1.call-done, bf16[512,2048]{1,0:T(8,128)(2,1)} %param.19, f32[2048]{0:T(1024)S(1)} %copy-done.33, f32[512]{0:T(512)S(1)} %copy-done.27), kind=kOutput, calls=%fused_computation.37 | convolution fusion | flops 2152202240 | bytes 7350272 | tf_op jit(solution)/shard_map/dot_general | solution.py:274
  384.5 3.1 reshape.416
  394.1 5.4 %fusion = (f32[4,4,2,128]{3,2,1,0:T(2,128)S(1)}, f32[4,4,384,128,2]{3,2,4,1,0:T(8,128)S(1)}) fusion(pred[4,128,384]{1,2,0:T(8,128)(4,1)S(1)} %copy-done.9, f32[4,128,4,2,128]{4,3,2,1,0:T(2,128)S(1)} %copy-done.7, bf16[4,128,4,2,32]{4,1,3,2,0:T(8,128)(2,1)} %copy.223, bf16[4,128,4,2,32]{4,1,3,2,0:T(8,128)(2,1)} %copy.222, ...), kind=kOutput, calls=%fused_computation.3 | convolution fusion | flops 418377728 | bytes 11747328 | tf_op jit(solution)/shard_map/kihgd,kjhd->khgij/dot_general | solution.py:93
  405.6 54.2 %all-gather.27.cloned.1.call-done = bf16[1024,2048]{1,0:T(8,128)(2,1)} async-done(((bf16[1024,512]{1,0:T(8,128)(2,1)}), bf16[1024,2048]{1,0:T(8,128)(2,1)}) %all-gather.27.cloned.1.call-update) | async-done | bytes 4194320 | tf_op jit(solution)/shard_map/all_gather | solution.py:271
  459.8 6.6 %fusion.130 = f32[512,2048]{1,0:T(8,128)} fusion(bf16[512,1024]{1,0:T(8,128)(2,1)S(1)} %convert_element_type.224, bf16[1024,2048]{1,0:T(8,128)(2,1)} %all-gather.27.cloned.1.call-done), kind=kOutput, calls=%fused_computation.233 | convolution fusion | flops 2147483648 | bytes 9437184 | tf_op jit(solution)/shard_map/dot_general | solution.py:378
  466.3 39.2 %all-gather.19.cloned.1.call-done = bf16[512,2048]{1,0:T(8,128)(2,1)} async-done(((bf16[512,512]{1,0:T(8,128)(2,1)}), bf16[512,2048]{1,0:T(8,128)(2,1)}) %all-gather.19.cloned.1.call-update) | async-done | bytes 2097168 | tf_op jit(solution)/shard_map/all_gather | solution.py:270
  505.5 5.5 %add_convert_fusion = bf16[512,2048]{1,0:T(8,128)(2,1)} fusion(f32[512,2048]{1,0:T(8,128)} %fusion.130, bf16[512,512]{0,1:T(8,128)(2,1)S(1)} %fusion.41, bf16[512,2048]{1,0:T(8,128)(2,1)} %all-gather.19.cloned.1.call-done), kind=kOutput, calls=%fused_computation.10 | convolution fusion | flops 1075838976 | bytes 8912896 | tf_op jit(solution)/shard_map/dot_general | solution.py:377
  511.0 8.7 %reduce-scatter.2.cloned.1.call-done = bf16[256,2048]{1,0:T(8,128)(2,1)} async-done(((bf16[512,2048]{1,0:T(8,128)(2,1)}), bf16[256,2048]{1,0:T(8,128)(2,1)}) %reduce-scatter.2.cloned.1.call-update) | async-done | bytes 1048592 | tf_op jit(solution)/shard_map/reduce_scatter | solution.py:375
  (209 shorter events, 80.2 us)
Async XLA Ops:
  6.5 9.7 %copy-start = (bf16[2048,16]{0,1:T(8,128)(2,1)S(1)}, bf16[2048,16]{0,1:T(8,128)(2,1)}, u32[]{:S(2)}) copy-start(bf16[2048,16]{0,1:T(8,128)(2,1)} %param.25) | copy-start | bytes 196612
  6.5 136.4 %all-gather.21.cloned.1.call-start = ((), (), s32[]{:S(2)}) async-start(), calls=%async_computation.5 | async-start | bytes 2621440 | tf_op jit(solution)/shard_map/all_gather | solution.py:268
  7.3 139.6 %all-gather.15.cloned.1.call-start = ((), (), s32[]{:S(2)}) async-start(), calls=%async_computation.2 | async-start | bytes 2621440 | tf_op jit(solution)/shard_map/all_gather | solution.py:265
  8.0 7.7 %copy-start.4 = (bf16[512,2048]{1,0:T(8,128)(2,1)S(1)}, bf16[512,2048]{1,0:T(8,128)(2,1)}, u32[]{:S(2)}) copy-start(bf16[512,2048]{1,0:T(8,128)(2,1)} %param.19) | copy-start | bytes 6291460
  8.0 174.6 %all-gather.13.cloned.1.call-start = ((), (), s32[]{:S(2)}) async-start(), calls=%async_computation.1 | async-start | bytes 2621440 | tf_op jit(solution)/shard_map/all_gather | solution.py:264
  8.8 228.4 %all-gather.23.cloned.1.call-start = ((), (), s32[]{:S(2)}) async-start(), calls=%async_computation.6 | async-start | bytes 2621440 | tf_op jit(solution)/shard_map/all_gather | solution.py:269
  9.3 313.9 %all-gather.17.cloned.1.call-start = ((), (), s32[]{:S(2)}) async-start(), calls=%async_computation.3 | async-start | bytes 2621440 | tf_op jit(solution)/shard_map/all_gather | solution.py:263
  9.9 369.2 %all-gather.25.cloned.1.call-start = ((), (), s32[]{:S(2)}) async-start(), calls=%async_computation.7 | async-start | bytes 5242880 | tf_op jit(solution)/shard_map/all_gather | solution.py:267
  10.5 449.2 %all-gather.27.cloned.1.call-start = ((), (), s32[]{:S(2)}) async-start(), calls=%async_computation.8 | async-start | bytes 5242880 | tf_op jit(solution)/shard_map/all_gather | solution.py:271
  11.3 494.2 %all-gather.19.cloned.1.call-start = ((), (), s32[]{:S(2)}) async-start(), calls=%async_computation.4 | async-start | bytes 2621440 | tf_op jit(solution)/shard_map/all_gather | solution.py:270
  11.3 44.2 %collective-permute-start = (bf16[1,512,512]{2,1,0:T(8,128)(2,1)}, bf16[1,512,512]{2,1,0:T(8,128)(2,1)}, u32[]{:S(2)}, u32[]{:S(2)}) collective-permute-start(bf16[1,512,512]{2,1,0:T(8,128)(2,1)} %bitcast.9), channel_id=1, source_target_pairs={{0,8},{8,0},{16,24},{24,16},{1,9},{9,1},{17,25},{25,17},{2,10},{10... | collective-permute-start | bytes 1572872 | tf_op jit(solution)/shard_map/ppermute | solution.py:29
  14.5 505.3 %reduce-scatter.2.cloned.1.call-start = ((), (), s32[]{:S(2)}) async-start(), calls=%async_computation.9 | async-start | bytes 3145728 | tf_op jit(solution)/shard_map/reduce_scatter | solution.py:375
  16.2 221.0 %copy-start.26 = (f32[512]{0:T(512)}, f32[512]{0:T(512)S(1)}, u32[]{:S(2)}) copy-start(f32[512]{0:T(512)S(1)} %add_rsqrt_fusion.1) | copy-start | bytes 6148
  58.5 80.0 %collective-permute-start.1 = (bf16[2,512,512]{2,1,0:T(8,128)(2,1)}, bf16[2,512,512]{2,1,0:T(8,128)(2,1)}, u32[]{:S(2)}, u32[]{:S(2)}) collective-permute-start(bf16[2,512,512]{2,1,0:T(8,128)(2,1)} %get-tuple-element.32), channel_id=1, source_target_pairs={{0,16},{8,24},{16,0},{24,8},{1,17},{9,25},{17,1},{25,9},{2,18},{10... | collective-permute-start | bytes 3145736 | tf_op jit(solution)/shard_map/ppermute | solution.py:29
  59.7 78.7 %copy-start.3 = (bf16[1,2,512,512]{3,2,1,0:T(8,128)(2,1)S(1)}, bf16[1,2,512,512]{3,2,1,0:T(8,128)(2,1)}, u32[]{:S(2)}) copy-start(bf16[1,2,512,512]{3,2,1,0:T(8,128)(2,1)} %get-tuple-element.31) | copy-start | bytes 3145732
  187.5 61.6 %collective-permute-start.2 = (bf16[2,1536]{0,1:T(8,128)(2,1)}, bf16[2,1536]{0,1:T(8,128)(2,1)}, u32[]{:S(2)}, u32[]{:S(2)}) collective-permute-start(bf16[2,1536]{0,1:T(8,128)(2,1)} %get-tuple-element.20), channel_id=1, source_target_pairs={{0,8},{8,16},{16,24},{1,9},{9,17},{17,25},{2,10},{10,18},{18,26},{... | collective-permute-start | bytes 18440 | tf_op jit(solution)/shard_map/ppermute | solution.py:48
  190.3 58.8 %collective-permute-start.3 = (bf16[2,1536]{0,1:T(8,128)(2,1)}, bf16[2,1536]{0,1:T(8,128)(2,1)}, u32[]{:S(2)}, u32[]{:S(2)}) collective-permute-start(bf16[2,1536]{0,1:T(8,128)(2,1)} %get-tuple-element.21), channel_id=1, source_target_pairs={{8,0},{16,8},{24,16},{9,1},{17,9},{25,17},{10,2},{18,10},{26,18},{... | collective-permute-start | bytes 18440 | tf_op jit(solution)/shard_map/ppermute | solution.py:50
  242.7 84.4 %collective-permute-start.4 = (bf16[128,1024]{0,1:T(8,128)(2,1)}, bf16[128,1024]{0,1:T(8,128)(2,1)S(1)}, u32[]{:S(2)}, u32[]{:S(2)}) collective-permute-start(bf16[128,1024]{0,1:T(8,128)(2,1)} %get-tuple-element.39), channel_id=1, source_target_pairs={{0,8},{8,16},{16,24},{1,9},{9,17},{17,25},{2,10},{10,18},{18,26},{... | collective-permute-start | bytes 786440 | tf_op jit(solution)/shard_map/ppermute | solution.py:48
  244.7 82.3 %collective-permute-start.5 = (bf16[128,1024]{0,1:T(8,128)(2,1)}, bf16[128,1024]{0,1:T(8,128)(2,1)}, u32[]{:S(2)}, u32[]{:S(2)}) collective-permute-start(bf16[128,1024]{0,1:T(8,128)(2,1)} %get-tuple-element.40), channel_id=1, source_target_pairs={{8,0},{16,8},{24,16},{9,1},{17,9},{25,17},{10,2},{18,10},{26,18},{... | collective-permute-start | bytes 786440 | tf_op jit(solution)/shard_map/ppermute | solution.py:50
  249.0 6.0 %copy-start.16 = (f32[1536]{0:T(1024)S(1)}, f32[1536]{0:T(1024)}, u32[]{:S(2)}) copy-start(f32[1536]{0:T(1024)} %get-tuple-element.8) | copy-start | bytes 18436
  249.0 6.0 %copy-start.17 = (f32[1536]{0:T(1024)S(1)}, f32[1536]{0:T(1024)}, u32[]{:S(2)}) copy-start(f32[1536]{0:T(1024)} %get-tuple-element.9) | copy-start | bytes 18436
  271.4 40.7 %copy-start.8 = (f32[4,4,128,128]{3,2,1,0:T(8,128)S(1)}, f32[4,4,128,128]{3,2,1,0:T(8,128)}, u32[]{:S(2)}) copy-start(f32[4,4,128,128]{3,2,1,0:T(8,128)} %fusion.58) | copy-start | bytes 3145732
  271.4 40.7 %copy-start.19 = (f32[4,4,2,128]{3,2,1,0:T(2,128)S(1)}, f32[4,4,2,128]{3,2,1,0:T(2,128)}, u32[]{:S(2)}) copy-start(f32[4,4,2,128]{3,2,1,0:T(2,128)} %copy.184) | copy-start | bytes 49156
  505.5 14.2 %copy-start.1 = (bf16[2048,16]{0,1:T(8,128)(2,1)S(1)}, bf16[2048,16]{0,1:T(8,128)(2,1)}, u32[]{:S(2)}) copy-start(bf16[2048,16]{0,1:T(8,128)(2,1)} %param.25) | copy-start | bytes 196612
  (26 other events, 84.3 us)
Sparse Core Ops, SparseCore 0:
  8.9 55.9 all-gather.20
  66.4 70.7 all-gather.14
  138.8 43.7 all-gather.12
  184.1 53.0 all-gather.22
  238.6 58.4 all-gather.16
  298.5 80.5 all-gather.24
  380.7 79.0 all-gather.26
  461.3 44.1 all-gather.18
  511.1 8.5 reduce-scatter.1
